TPU v7x, 32 devices: a whole 2x2x4 slice. The times are simulated.
32 devices in a mesh: ep: 8 (over z, y), tp: 4 (over x, core).
Axes of the slice: x: 2, y: 2, z: 4, core: 2. Of those that a mesh axis runs over, the one named last changes fastest.
Arguments:
- queries: bfloat16 [4096, 512], P('ep', 'tp'), may hold values from -6 to 6
- key_rows: bfloat16 [4096, 512], P('ep', 'tp'), may hold values from -6 to 6
- value_rows: bfloat16 [4096, 1024], P('ep', 'tp'), may hold values from -6 to 6
- forget_gate_input: bfloat16 [4096, 512], P('ep', 'tp'), may hold values from -6 to 6
- channel_decay_rate: float32 [512], P('tp'), may hold values from 0 to 1, as said below
- position_decay_factor: float32 [4096], P('ep'), may hold values from 0 to 3, as said below
- extra_log_decay: float32 [4096, 8], P('ep', 'tp'), may hold values from -1 to 0, as said below
- head_norm_gain: float32 [8, 128], P('tp'), may hold values from 0.1 to 1.9
- output_projection_weight: bfloat16 [1024, 2048], P('tp'), may hold values from -0.1875 to 0.1875
- expert_input_rows: bfloat16 [2048, 2048], P('ep'), may hold values from -6 to 6
- expert_norm_gain: float32 [2048], replicated, may hold values from 0.1 to 1.9
- routes: int32 [2048, 2], P('ep'), may hold values from 0 to 7, all different within a row; in each aligned block of 256 rows (0 to 255, 256 to 511, ...) at most 128 rows name the same one
- chosen_expert_weights: float32 [2048, 2], P('ep'), may hold values from 0.2 to 1
- expert_gate_weight: bfloat16 [8, 2048, 3072], P('ep', None, 'tp'), may hold values from -0.125 to 0.125
- expert_up_weight: bfloat16 [8, 2048, 3072], P('ep', None, 'tp'), may hold values from -0.125 to 0.125
- expert_down_weight: bfloat16 [8, 3072, 2048], P('ep', 'tp'), may hold values from -0.109375 to 0.109375
Outputs:
- token_mixer_output: bfloat16 [4096, 2048], P(('ep', 'tp'))
- moe_out: bfloat16 [2048, 2048], P('ep', 'tp')
Inputs may be any that keep to these rules, and one draw needn't show every extreme that they name: `routes`: within the rows of one device no expert is named by more than 128 of the choices, a bound that some block reaches; the 2 experts of a token differ. `channel_decay_rate`: Positive. `position_decay_factor`: Positive. `extra_log_decay`: zero or negative.
All inputs are finite; a program needn't handle non-finite values.
Results may differ from a plain program's by a relative error of at most 0.019.
Values may be sent and summed in bfloat16 or wider, within the bound.
A program may use at most 128 MiB of HBM per device.

v0:
```python
import jax
import jax.numpy as jnp
from jax import lax
from jax.sharding import PartitionSpec as P

KEY_CHANNELS = 64
VALUE_DIM = 128
SPAN = 64


highest_precision = lax.Precision.HIGHEST
norm_eps = 1e-06


def prefix(value, axis, combine, identity):
    peers, index = (lax.axis_size(axis), lax.axis_index(axis))
    everything = jax.tree.map(
        lambda part, kind: lax.all_gather(part.astype(kind), axis),
        value,
        (jnp.bfloat16, jnp.bfloat16),
    )
    start = jax.tree.map(
        lambda part, zero: jnp.broadcast_to(jnp.asarray(zero, part.dtype), part.shape),
        value,
        identity,
    )

    def hop(k, before):
        reached = k < index
        new = combine(
            before, jax.tree.map(lambda part, own: part[k].astype(own.dtype), everything, value)
        )
        return jax.tree.map(lambda a, b: jnp.where(reached, a, b), new, before)

    return lax.fori_loop(0, peers, hop, start)


def gla_blocks(query_single, key_float, value_float, decay_logarithm, span_rows):
    length, head_count, key_width = query_single.shape
    value_width = value_float.shape[-1]
    block_count = length // span_rows

    def blocked(tensor):
        return tensor.reshape(block_count, span_rows, head_count, tensor.shape[-1])

    causal = (jnp.arange(span_rows)[:, None] >= jnp.arange(span_rows)[None, :])[:, :, None, None]

    def advance(carried_state, pieces):
        block_queries, block_keys, block_values, gate_block = pieces
        cumulative_decay = jnp.cumsum(gate_block, axis=0)
        log_gaps = cumulative_decay[:, None] - cumulative_decay[None, :]
        decays = jnp.exp(jnp.where(causal, log_gaps, -jnp.inf))
        scores = jnp.sum(block_queries[:, None] * block_keys[None, :] * decays, axis=-1)
        final_output = jnp.einsum("ijh,jhv->ihv", scores, block_values, precision=highest_precision)
        final_output = final_output + jnp.einsum(
            "nwt,wto->nwo",
            block_queries * jnp.exp(cumulative_decay),
            carried_state,
            precision=highest_precision,
        )
        final_log_decay = cumulative_decay[-1]
        carried_state = jnp.exp(final_log_decay)[:, :, None] * carried_state + jnp.einsum(
            "ygc,yga->gca",
            block_keys * jnp.exp(final_log_decay[None] - cumulative_decay),
            block_values,
            precision=highest_precision,
        )
        return (carried_state, final_output)

    start_state = jnp.zeros((head_count, key_width, value_width), jnp.float32)
    carried_state, outputs = lax.scan(
        advance,
        start_state,
        (blocked(query_single), blocked(key_float), blocked(value_float), blocked(decay_logarithm)),
    )
    return (outputs.reshape(length, head_count, value_width), carried_state)


def combine_states(earlier, latter):
    return (earlier[0] * latter[0], latter[0][:, :, None] * earlier[1] + latter[1])


def mixer_part(
    queries,
    key_rows,
    value_rows,
    forget_gate_input,
    channel_decay_rate,
    position_decay_factor,
    extra_log_decay,
    head_norm_gain,
    output_projection_weight,
):
    length = queries.shape[0]
    head_count = head_norm_gain.shape[0]
    query_single = queries.astype(jnp.float32).reshape(length, head_count, KEY_CHANNELS)
    key_float = key_rows.astype(jnp.float32).reshape(length, head_count, KEY_CHANNELS)
    value_float = value_rows.astype(jnp.float32).reshape(length, head_count, VALUE_DIM)
    gate_logarithm = jax.nn.log_sigmoid(forget_gate_input.astype(jnp.float32)).reshape(
        length, head_count, KEY_CHANNELS
    )
    decay_logarithm = (
        gate_logarithm
        * channel_decay_rate.reshape(head_count, KEY_CHANNELS)[None]
        * position_decay_factor[:, None, None]
        + extra_log_decay[:, :, None]
    )
    local_out, local_state = gla_blocks(query_single, key_float, value_float, decay_logarithm, SPAN)
    cumulative_decay = jnp.cumsum(decay_logarithm, axis=0)
    total_decay = jnp.exp(cumulative_decay[-1])
    identity = (jnp.ones_like(total_decay), jnp.zeros_like(local_state))
    incoming_state = prefix((total_decay, local_state), "ep", combine_states, identity)
    mixed_out = local_out + jnp.einsum(
        "pmj,mjx->pmx",
        query_single * jnp.exp(cumulative_decay),
        incoming_state[1],
        precision=highest_precision,
    )
    scale = lax.rsqrt(jnp.mean(mixed_out * mixed_out, axis=-1, keepdims=True) + norm_eps)
    head_normed = (
        (mixed_out * scale * head_norm_gain[None])
        .astype(jnp.bfloat16)
        .reshape(length, head_count * VALUE_DIM)
    )
    return lax.psum_scatter(
        jnp.dot(head_normed, output_projection_weight, preferred_element_type=jnp.float32).astype(
            jnp.bfloat16
        ),
        "tp",
        scatter_dimension=0,
        tiled=True,
    )


def expert_part(
    expert_input_rows,
    expert_norm_gain,
    routes,
    chosen_expert_weights,
    expert_gate_weight,
    expert_up_weight,
    expert_down_weight,
):
    token_count = expert_input_rows.shape[0]
    model_width = expert_input_rows.shape[1]
    top_count = routes.shape[1]
    rows_float = expert_input_rows.astype(jnp.float32)
    scaled = rows_float * lax.rsqrt(
        jnp.mean(rows_float * rows_float, axis=-1, keepdims=True) + norm_eps
    )
    moe_normed = (scaled * expert_norm_gain[None]).astype(jnp.bfloat16)
    expert_count = lax.axis_size("ep")
    capacity = 4 * token_count // expert_count
    flat_routes = routes.reshape(-1)
    onehot = (flat_routes[:, None] == jnp.arange(expert_count, dtype=jnp.int32)[None, :]).astype(
        jnp.int32
    )
    slot_ranks = jnp.cumsum(onehot, axis=0) - 1
    slot_index = jnp.sum(slot_ranks * onehot, axis=1)
    position = flat_routes * capacity + slot_index
    token_index = jnp.arange(token_count * top_count, dtype=jnp.int32) // top_count
    gate_weight = expert_gate_weight[0]
    up_weight = expert_up_weight[0]
    down_weight = expert_down_weight[0]
    quarter = model_width // lax.axis_size("tp")
    columns = lax.dynamic_slice_in_dim(moe_normed, lax.axis_index("tp") * quarter, quarter, 1)
    buffer = (
        jnp.zeros((expert_count * capacity, quarter), jnp.bfloat16)
        .at[position]
        .set(columns[token_index])
    )
    buffer = buffer.reshape(expert_count, capacity, quarter)
    pieces = lax.all_gather(
        lax.all_to_all(buffer, "ep", split_axis=0, concat_axis=0, tiled=True),
        "tp",
        axis=2,
        tiled=True,
    )
    gate_sum = jnp.einsum("sid,df->sif", pieces, gate_weight, preferred_element_type=jnp.float32)
    up_sum = jnp.einsum("sid,df->sif", pieces, up_weight, preferred_element_type=jnp.float32)
    partial_value = jnp.einsum(
        "sif,fd->sid",
        (jax.nn.silu(gate_sum) * up_sum).astype(jnp.bfloat16),
        down_weight,
        preferred_element_type=jnp.float32,
    )
    summed = lax.psum_scatter(
        partial_value.astype(jnp.bfloat16), "tp", scatter_dimension=2, tiled=True
    )
    returned = lax.all_to_all(summed, "ep", split_axis=0, concat_axis=0, tiled=True)
    flat_rows = returned.reshape(expert_count * capacity, returned.shape[2])
    picked = (
        flat_rows[position].astype(jnp.float32).reshape(token_count, top_count, returned.shape[2])
    )
    return jnp.sum(picked * chosen_expert_weights[:, :, None], axis=1).astype(jnp.bfloat16)


def body(
    queries,
    key_rows,
    value_rows,
    forget_gate_input,
    channel_decay_rate,
    position_decay_factor,
    extra_log_decay,
    head_norm_gain,
    output_projection_weight,
    expert_input_rows,
    expert_norm_gain,
    routes,
    chosen_expert_weights,
    expert_gate_weight,
    expert_up_weight,
    expert_down_weight,
):
    token_mixer_output = mixer_part(
        queries,
        key_rows,
        value_rows,
        forget_gate_input,
        channel_decay_rate,
        position_decay_factor,
        extra_log_decay,
        head_norm_gain,
        output_projection_weight,
    )
    moe_out = expert_part(
        expert_input_rows,
        expert_norm_gain,
        routes,
        chosen_expert_weights,
        expert_gate_weight,
        expert_up_weight,
        expert_down_weight,
    )
    return (token_mixer_output, moe_out)


def solution(mesh):
    return jax.shard_map(
        body,
        mesh=mesh,
        in_specs=(
            P("ep", "tp"),
            P("ep", "tp"),
            P("ep", "tp"),
            P("ep", "tp"),
            P("tp"),
            P("ep"),
            P("ep", "tp"),
            P("tp", None),
            P("tp", None),
            P("ep", None),
            P(),
            P("ep", None),
            P("ep", None),
            P("ep", None, "tp"),
            P("ep", None, "tp"),
            P("ep", "tp", None),
        ),
        out_specs=(P(("ep", "tp"), None), P("ep", "tp")),
        check_vma=False,
    )
```

profile of v0, /device:TPU:0, one launch (start us, length us, event | category | flops | bytes accessed | tf_op | source)
XLA Modules:
  0.0 284.9 jit_solution(6712470127259616729)
XLA Ops:
  7.2 3.0 %convert_element_type.79 = f32[256,2048]{1,0:T(8,128)} convert(bf16[256,2048]{1,0:T(8,128)(2,1)} %param.29) | non-fusion elementwise | flops 524288 | bytes 3145728 | tf_op jit(solution)/shard_map/convert_element_type | solution.py:147
  14.8 5.8 %scatter_custom_fusion = bf16[1024,512]{1,0:T(8,128)(2,1)} fusion(s32[512]{0:T(512)S(1)} %bitcast.145, bf16[256,512]{1,0:T(8,128)(2,1)S(1)} %fusion.30, s32[1024]{0:T(1024)S(1)} %pad_clamp_fusion.1, bf16[]{:T(256)} %constant.98.clone.1), kind=kCustom, calls=%fused_computation.51 | custom fusion | bytes 1048578 | tf_op jit(solution)/shard_map/scatter | solution.py:170
  20.6 33.3 %all_to_all.10 = bf16[8,128,512]{2,1,0:T(8,128)(2,1)} all-to-all(bf16[8,128,512]{2,1,0:T(8,128)(2,1)} %bitcast.137), channel_id=1, replica_groups=mesh['ep'=8,'tp'=4] {'ep'}, dimensions={0} | all-to-all | bytes 2097152 | tf_op jit(solution)/shard_map/all_to_all | solution.py:174
  57.8 2.1 copy.69
  62.5 1.9 reshape_reshape.19
  64.4 2.0 reshape.205
  66.4 2.0 reshape.206
  68.4 2.9 %multiply_add_fusion = f32[8,64,2,64]{3,2,1,0:T(2,128)} fusion(f32[8,64,2,64]{3,2,1,0:T(2,128)} %copy.69, f32[8,64,2]{2,1,0:T(8,128)} %bitcast.141, f32[8,64]{1,0:T(8,128)S(1)} %mul.165, f32[2,64]{1,0:T(2,128)S(1)} %mul.162), kind=kLoop, calls=%fused_computation.56 | loop fusion | flops 196608 | bytes 530944 | tf_op jit(solution)/shard_map/add | solution.py:103
  71.3 16.3 %all-gather.3.cloned.1.call-done = bf16[8,128,2048]{2,1,0:T(8,128)(2,1)} async-done(((bf16[8,128,512]{2,1,0:T(8,128)(2,1)}), bf16[8,128,2048]{2,1,0:T(8,128)(2,1)}) %all-gather.3.cloned.1.call-update) | async-done | bytes 4194320 | tf_op jit(solution)/shard_map/all_gather | solution.py:173
  87.6 8.3 %fusion.20 = f32[8,128,768]{2,1,0:T(8,128)} fusion(bf16[8,128,2048]{2,1,0:T(8,128)(2,1)} %all-gather.3.cloned.1.call-done, bf16[1,2048,768]{2,1,0:T(8,128)(2,1)} %param.34), kind=kOutput, calls=%fused_computation.37 | convolution fusion | flops 3221225472 | bytes 10485760 | tf_op jit(solution)/shard_map/sid,df->sif/dot_general | solution.py:180
  95.9 12.3 %convolution_convert_fusion = bf16[8,128,2048]{2,1,0:T(8,128)(2,1)} fusion(bf16[1,768,2048]{2,1,0:T(8,128)(2,1)S(1)} %copy-done, f32[8,128,768]{2,1,0:T(8,128)} %fusion.20, bf16[8,128,2048]{2,1,0:T(8,128)(2,1)} %all-gather.3.cloned.1.call-done, bf16[1,2048,768]{2,1,0:T(8,128)(2,1)} %param.33), kind=kOutput, calls=%fused_computation.35 | convolution fusion | flops 6449266688 | bytes 17825792 | tf_op jit(solution)/shard_map/sif,fd->sid/dot_general | solution.py:181
  108.3 59.1 %while.27 = (s32[]{:T(128)}, f32[2,64,128]{2,1,0:T(8,128)S(1)}, f32[8,64,2,128]{3,1,0,2:T(8,128)}, f32[8,64,2,64]{3,2,1,0:T(2,128)}, f32[8,64,2,64]{3,2,1,0:T(2,...) while((s32[]{:T(128)}, f32[2,64,128]{2,1,0:T(8,128)S(1)}, ...), condition=%wide.region_3.4_spmd.clone, body=%wide.region_0.3_spmd.clone.sunk | while | flops 40988672 | bytes 1486964 | solution.py:71
  111.4 2.0 multiply_reduce_fusion.5
  118.9 2.0 multiply_reduce_fusion.5
  126.3 2.0 multiply_reduce_fusion.5
  133.7 2.0 multiply_reduce_fusion.5
  141.1 2.0 multiply_reduce_fusion.5
  148.4 2.0 multiply_reduce_fusion.5
  155.8 2.0 multiply_reduce_fusion.5
  163.2 2.0 multiply_reduce_fusion.5
  170.9 4.5 %reduce-window.14 = f32[64,2,4,128]{3,0,1,2:T(8,128)S(1)} reduce-window(f32[64,2,4,128]{3,0,1,2:T(8,128)} %copy_bitcast_fusion.3, f32[]{:T(128)} %constant.93.clone.1), window={size=1x1x1x128 pad=0_0x0_0x0_0x127_0}, to_apply=%region_4.5 | reduce-window | flops 8323072 | bytes 524292 | tf_op jit(solution)/shard_map/reduce-window
  179.7 2.0 copy.80
  181.8 20.6 %all_gather.13 = bf16[8,2,64]{2,1,0:T(2,128)(2,1)S(1)} all-gather(bf16[1,2,64]{2,1,0:T(2,128)(2,1)S(1)} %exponential_convert_fusion), channel_id=1, replica_groups=mesh['ep'=8,'tp'=4] {'ep'}, dimensions={0}, use_global_device_ids=true | all-gather | bytes 2304 | tf_op jit(solution)/shard_map/all_gather | solution.py:18
  202.4 32.9 %all-gather = bf16[16,64,128]{2,1,0:T(8,128)(2,1)} all-gather(bf16[2,64,128]{2,1,0:T(8,128)(2,1)} %convert_element_type.75), channel_id=2, replica_groups=mesh['ep'=8,'tp'=4] {'ep'}, dimensions={0}, use_global_device_ids=true | all-gather | bytes 294912 | tf_op jit(solution)/shard_map/all_gather | solution.py:18
  235.3 7.2 %while.28 = (s32[]{:T(128)}, f32[2,64,128]{2,1,0:T(8,128)S(1)}, s32[]{:T(128)}, bf16[8,2,64]{2,1,0:T(2,128)(2,1)S(1)}, bf16[8,2,64,128]{3,2,1,0:T(8,128)(2,1)}, /*index=5*/s32[]{:T(128)}, s32[]{:T(128)}) while((s32[]{:T(128)}, f32[2,64,128]{2,1,0:T(8,128)S(1)}, s32[]{:T(128)}, bf16[8,2,64]{2,1,0:T(2,128)(2,1)S(1)}, ...), condition=%wide.region_7.8_spmd.clone, body=%wide.region_6.7_spmd.clone.sunk | while | flops 82052 | bytes 165225 | solution.py:35
  242.5 2.0 multiply_reduce_fusion.3
  245.3 2.1 convolution_convert_fusion.1
  247.4 4.5 %all-to-all-start.1 = ((bf16[8,128,512]{2,1,0:T(8,128)(2,1)}), bf16[8,128,512]{2,1,0:T(8,128)(2,1)}, u32[]{:S(2)}, u32[]{:S(2)}) async-start(bf16[8,128,512]{2,1,0:T(8,128)(2,1)} %reduce-scatter.5.cloned.1.call-done), calls=%async_computation.3 | async-start | bytes 2097152 | tf_op jit(solution)/shard_map/all_to_all | solution.py:190
  252.0 16.3 %all-to-all-done.1 = bf16[8,128,512]{2,1,0:T(8,128)(2,1)} async-done(((bf16[8,128,512]{2,1,0:T(8,128)(2,1)}), bf16[8,128,512]{2,1,0:T(8,128)(2,1)}, u32[]{:S(2)}, u32[]{:S(2)}) %all-to-all-start.1) | async-done | bytes 1048608 | tf_op jit(solution)/shard_map/all_to_all | solution.py:190
  268.4 4.0 %gather_fusion = bf16[512,512]{1,0:T(8,128)(2,1)} fusion(bf16[1024,512]{1,0:T(8,128)(2,1)} %bitcast.22, s32[1024]{0:T(1024)S(1)} %pad_clamp_fusion), kind=kCustom, calls=%fused_computation.1 | custom fusion | bytes 1050624 | tf_op jit(solution)/shard_map/gather | solution.py:193
  272.4 2.7 reshape.207
  275.1 3.3 %multiply_reduce_fusion.2 = bf16[256,512]{1,0:T(8,128)(2,1)} fusion(f32[256,2,512]{2,1,0:T(2,128)} %reshape.207, f32[256,2]{1,0:T(8,128)S(1)} %copy.84), kind=kLoop, calls=%fused_computation.46 | loop fusion | flops 393216 | bytes 1312768 | tf_op jit(solution)/shard_map/reduce_sum | solution.py:195
  (191 shorter events, 68.7 us)
Async XLA Ops:
  7.2 88.8 %copy-start = (bf16[1,768,2048]{2,1,0:T(8,128)(2,1)S(1)}, bf16[1,768,2048]{2,1,0:T(8,128)(2,1)}, u32[]{:S(2)}) copy-start(bf16[1,768,2048]{2,1,0:T(8,128)(2,1)} %param.35) | copy-start | bytes 9437188
  7.2 3.3 %copy-start.7 = (s32[256,2]{0,1:T(2,128)S(1)}, s32[256,2]{0,1:T(2,128)}, u32[]{:S(2)}) copy-start(s32[256,2]{0,1:T(2,128)} %param.31) | copy-start | bytes 6148
  7.2 80.4 %all-gather.3.cloned.1.call-start = ((), (), s32[]{:S(2)}) async-start(), calls=%async_computation.5 | async-start | bytes 5242880 | tf_op jit(solution)/shard_map/all_gather | solution.py:173
  7.2 3.0 %copy-start.1 = (bf16[256,2048]{1,0:T(8,128)(2,1)S(1)}, bf16[256,2048]{1,0:T(8,128)(2,1)}, u32[]{:S(2)}) copy-start(bf16[256,2048]{1,0:T(8,128)(2,1)} %param.29) | copy-start | bytes 3145732
  10.5 43.7 %copy-start.4 = (bf16[512,128]{1,0:T(8,128)(2,1)S(1)}, bf16[512,128]{1,0:T(8,128)(2,1)}, u32[]{:S(2)}) copy-start(bf16[512,128]{1,0:T(8,128)(2,1)} %param.23) | copy-start | bytes 393220
  14.8 45.1 %copy-start.5 = (f32[512,2]{0,1:T(2,128)S(1)}, f32[512,2]{0,1:T(2,128)}, u32[]{:S(2)}) copy-start(f32[512,2]{0,1:T(2,128)} %param.26) | copy-start | bytes 12292
  20.6 40.1 %copy-start.6 = (f32[512]{0:T(512)S(1)}, f32[512]{0:T(512)}, u32[]{:S(2)}) copy-start(f32[512]{0:T(512)} %param.25) | copy-start | bytes 6148
  54.0 193.4 %reduce-scatter.5.cloned.1.call-start = ((), (), s32[]{:S(2)}) async-start(), calls=%async_computation.6 | async-start | bytes 5242880 | tf_op jit(solution)/shard_map/reduce_scatter | solution.py:187
  56.8 39.1 %copy-start.2 = (f32[512,128]{0,1:T(8,128)}, f32[512,128]{0,1:T(8,128)S(1)}, u32[]{:S(2)}) copy-start(f32[512,128]{0,1:T(8,128)S(1)} %fusion.34) | copy-start | bytes 786436
  108.3 170.1 %reduce-scatter.3.cloned.1.call-start = ((), (), s32[]{:S(2)}) async-start(), calls=%async_computation.4 | async-start | bytes 2621440 | tf_op jit(solution)/shard_map/reduce_scatter | solution.py:125
  242.5 2.8 copy-start.3
  247.3 4.5 %copy-start.8 = (f32[256,2]{0,1:T(2,128)S(1)}, f32[256,2]{0,1:T(2,128)}, u32[]{:S(2)}) copy-start(f32[256,2]{0,1:T(2,128)} %param.32) | copy-start | bytes 6148
  247.4 21.0 %all-to-all-start.1 = ((bf16[8,128,512]{2,1,0:T(8,128)(2,1)}), bf16[8,128,512]{2,1,0:T(8,128)(2,1)}, u32[]{:S(2)}, u32[]{:S(2)}) async-start(bf16[8,128,512]{2,1,0:T(8,128)(2,1)} %reduce-scatter.5.cloned.1.call-done), calls=%async_computation.3 | async-start | bytes 2097152 | tf_op jit(solution)/shard_map/all_to_all | solution.py:190
Sparse Core Ops, SparseCore 0:
  54.1 33.4 all-gather.2
  108.4 44.3 reduce-scatter.4
  247.5 27.4 reduce-scatter.2
where the time goes:
time: 288 us; the launch traced here: 285 us
  blocking collectives  86.8 us (30%)
  other arithmetic  60.8 us (21%)
  local copies, waits for them, and re-layouts  49.7 us (17%)
  matrix products  35.3 us (12%)
  waiting for transfers between devices  32.7 us (11%)
  between operations  14 us (5%)
  starting transfers between devices  4.77 us (2%)
    all_gather x2, blocking collectives, prefix(): lax.all_gather(part.astype(kind), axis)  53.5 us
    all_to_all x1, blocking collectives, expert_part(): lax.all_to_all(buffer, 'ep', split_axis=0, concat_axis=0, tiled=True)  33.3 us
    dynamic_slice x24, local copies, waits for them, and re-layouts, gla_blocks(): lax.scan(advance, start_state, (blocked(query_single), blocked(key_float)...  16.4 us
    reduce_sum x8, other arithmetic, advance(): jnp.sum(block_queries[:, None] * block_keys[None, :] * decays, axis=-1)  16.4 us
    all_to_all x1, waiting for transfers between devices, expert_part(): lax.all_to_all(summed, 'ep', split_axis=0, concat_axis=0, tiled=True)  16.3 us
    all_gather x1, waiting for transfers between devices, expert_part(): lax.all_gather(lax.all_to_all(buffer, 'ep', split_axis=0, concat_axis=0,...  16.3 us
    dot_general x1, matrix products, expert_part(): jnp.einsum('sif,fd->sid', (jax.nn.silu(gate_sum) * up_sum).astype(jnp.bfl...  12.3 us
    dot_general x1, matrix products, expert_part(): jnp.einsum('sid,df->sif', pieces, up_weight, preferred_element_type=jnp.f...  8.33 us
  transfers between devices with their start and end apart: 4, of which 2 were waited for; matrix products, arithmetic and copies ran while one was open for 39% of the time, Pallas kernels for 0%

commit v1 on v0

v1 whole, which is shorter than its diff:
```python
import functools

import jax
import jax.numpy as jnp
from jax import lax
from jax.experimental import pallas as pl
from jax.experimental.pallas import tpu as pltpu
from jax.sharding import PartitionSpec as P

EPS = 1e-06
CHUNK = 128
GROUP_ROWS = 256
BF = jnp.bfloat16
F32 = jnp.float32
MESH = pl.DeviceIdType.MESH


def flip(a, b, size):
    total = 0
    bit = 1
    while bit < size:
        total = total + ((a // bit) % 2 + (b // bit) % 2) % 2 * bit
        bit *= 2
    return total


def dot(a, b, dims=((1,), (0,))):
    return lax.dot_general(a, b, (dims, ((), ())), preferred_element_type=F32)


def iota(shape, dim):
    return lax.broadcasted_iota(jnp.int32, shape, dim)


def level_sums(half):
    i, t = iota((CHUNK, CHUNK), 0), iota((CHUNK, CHUNK), 1)
    step = 2 * half
    same = (i // step) == (t // step)
    upper_i, upper_t = (i % step) >= half, (t % step) >= half
    return same & ((upper_i & upper_t & (t <= i)) | (~upper_i & ~upper_t & (t > i)))


def level_pairs(half):
    i, j = iota((CHUNK, CHUNK), 0), iota((CHUNK, CHUNK), 1)
    step = 2 * half
    return ((i // step) == (j // step)) & ((i % step) >= half) & ((j % step) < half)


def kernel(
    ep, tp,
    q_ref, k_ref, v_ref, f_ref, rate_ref, aux_ref, hgain_ref, x_ref, xgain_ref, routes_ref, w_ref,
    wo_hbm, wg_hbm, wu_hbm, wd_hbm,
    out1, out2,
    disp, recv, psend, pkeep, precv, xsum, xrecv, fin, ret, hot,
    sums, oloc, qin, state, ssend, srecv, dsend, drecv, hn,
    msend, mkeep, mprecv, mxsum, mxrecv,
    wo, wg, wu, wd,
    ep_s, ep_r, x_s, x_r, p_s, p_r, r_s, r_r,
    fp_s, fp_r, fx_s, fx_r, b_s, b_r,
    st_s, st_r, dc_s, dc_r,
    mp_s, mp_r, mx_s, mx_r, w_s,
):
    me, col = lax.axis_index("ep"), lax.axis_index("tp")
    partner = col + 1 - 2 * (col % 2)
    across = (col + 2) % tp
    diagonal = (partner + 2) % tp
    tokens, quarter = out2.shape
    slots = disp.shape[0]
    cap = slots // ep
    group = min(GROUP_ROWS, slots)
    per_group = group // cap
    groups = slots // group
    length = q_ref.shape[0]
    chunks = length // CHUNK
    values = v_ref.shape[1] // 2
    rows_out = out1.shape[0]

    def remote(src, dst, s, r, **where):
        return pltpu.make_async_remote_copy(
            src_ref=src, dst_ref=dst, send_sem=s, recv_sem=r, device_id=where, device_id_type=MESH
        )

    loads = [
        pltpu.make_async_copy(a, b, w_s.at[n])
        for n, (a, b) in enumerate(((wg_hbm.at[0], wg), (wu_hbm.at[0], wu), (wd_hbm.at[0], wd), (wo_hbm, wo)))
    ]
    for load in loads:
        load.start()

    barrier = pltpu.get_barrier_semaphore()
    for d in range(1, ep):
        pl.semaphore_signal(barrier, inc=1, device_id={"ep": flip(me, d, ep)}, device_id_type=MESH)
    for peer in (partner, across):
        pl.semaphore_signal(barrier, inc=1, device_id={"tp": peer}, device_id_type=MESH)

    lower = (iota((tokens, tokens), 0) <= iota((tokens, tokens), 1)).astype(BF)
    expert = iota((ep, tokens), 0)
    first_slot = flip(expert, me, ep) * cap - 1
    before = jnp.zeros((ep, 1), F32)
    for choice in range(2):
        named = expert == routes_ref[choice : choice + 1, :]
        rank = dot(named.astype(F32).astype(BF), lower) + before
        place = jnp.sum(jnp.where(named, rank.astype(jnp.int32) + first_slot, 0), axis=0, keepdims=True)
        before = rank[:, tokens - 1 : tokens]
        hot[choice] = (iota((slots, tokens), 0) == place).astype(F32).astype(BF)
    rows = x_ref[...].astype(F32)
    scale = lax.rsqrt(jnp.mean(rows * rows, axis=-1, keepdims=True) + EPS)
    columns = pl.ds(pl.multiple_of(col * quarter, quarter), quarter)
    normed = (x_ref[:, columns].astype(F32) * scale * xgain_ref[:, columns]).astype(BF)
    for g in range(groups):
        span = pl.ds(g * group, group)
        disp[span, :] = dot(hot[0, span, :] + hot[1, span, :], normed).astype(BF)
    recv[col, pl.ds(0, cap), :] = disp[0:cap, :]

    pl.semaphore_wait(barrier, ep + 1)

    def block(d):
        return pl.ds(d * cap, cap)

    def to_expert(d):
        return remote(disp.at[block(d)], recv.at[col, block(d)], ep_s.at[d], ep_r.at[d], ep=flip(me, d, ep))

    def over(d):
        return remote(recv.at[col, block(d)], recv.at[col, block(d)], x_s.at[d], x_r.at[d], tp=across)

    def over_in(d):
        return remote(recv.at[across, block(d)], recv.at[across, block(d)], x_s.at[d], x_r.at[d], tp=across)

    def beside(d):
        return remote(recv.at[col, block(d)], recv.at[col, block(d)], p_s.at[d], p_r.at[d], tp=partner)

    def beside_in(d):
        return remote(recv.at[partner, block(d)], recv.at[partner, block(d)], p_s.at[d], p_r.at[d], tp=partner)

    def relay(d):
        return remote(recv.at[across, block(d)], recv.at[across, block(d)], r_s.at[d], r_r.at[d], tp=partner)

    def relay_in(d):
        return remote(recv.at[diagonal, block(d)], recv.at[diagonal, block(d)], r_s.at[d], r_r.at[d], tp=partner)

    for d in range(1, ep):
        to_expert(d).start()

    def forward(d):
        if d:
            to_expert(d).wait_recv()
        over(d).start()
        beside(d).start()

    def pass_on(d):
        over_in(d).wait_recv()
        relay(d).start()

    forward(0)

    halves = []
    half = CHUNK // 2
    while half:
        halves.append(half)
        half //= 2
    count = len(halves)
    for n, h in enumerate(halves):
        sums[n * CHUNK : (n + 1) * CHUNK, :] = level_sums(h).astype(F32).astype(BF)
    ci, ct = iota((CHUNK, CHUNK), 0), iota((CHUNK, CHUNK), 1)
    sums[count * CHUNK : (count + 1) * CHUNK, :] = (ct <= ci).astype(F32).astype(BF)
    sums[(count + 1) * CHUNK : (count + 2) * CHUNK, :] = (ct > ci).astype(F32).astype(BF)
    width = q_ref.shape[1]
    lane = iota((CHUNK, width), 1)
    head_of = [(lane < width // 2).astype(F32), (lane >= width // 2).astype(F32)]
    ones = jnp.ones((CHUNK, values), BF)
    state[...] = jnp.zeros_like(state)
    so_far = [jnp.zeros((1, width), F32)]

    def recur(c):
        at = pl.ds(c * CHUNK, CHUNK)
        gate = f_ref[at, :].astype(F32)
        log_gate = jnp.minimum(gate, 0.0) - jnp.log1p(jnp.exp(-jnp.abs(gate)))
        extra = jnp.where(lane < width // 2, aux_ref[at, 1:2], aux_ref[at, 2:3])
        decay = log_gate * rate_ref[...] * aux_ref[at, 0:1] + extra
        high = decay.astype(BF)
        low = (decay - high.astype(F32)).astype(BF)
        logs = dot(sums[...], high) + dot(sums[...], low)
        q, k = q_ref[at, :].astype(F32), k_ref[at, :].astype(F32)

        def both(a):
            return jnp.concatenate([a * head_of[0], a * head_of[1]], axis=0).astype(BF)

        def scores(a, b, mask):
            s = dot(both(a), b.astype(BF), ((1,), (1,)))
            return [jnp.where(mask, s[:CHUNK], 0.0), jnp.where(mask, s[CHUNK:], 0.0)]

        total = scores(q, k, ci == ct)
        for n, h in enumerate(halves):
            e = jnp.exp(logs[n * CHUNK : (n + 1) * CHUNK])
            part = scores(q * e, k * e, level_pairs(h))
            total = [total[0] + part[0], total[1] + part[1]]
        prefix = logs[count * CHUNK : (count + 1) * CHUNK]
        suffix = logs[(count + 1) * CHUNK :]
        held = state[...].astype(BF)
        carried = dot(both(q * jnp.exp(prefix)), held)
        key_end = k * jnp.exp(suffix)
        new = jnp.exp(dot(high, ones, ((0,), (0,))) + dot(low, ones, ((0,), (0,)))) * state[...]
        for head in range(2):
            v = v_ref[at, head * values : (head + 1) * values]
            oloc[at, head * values : (head + 1) * values] = (
                dot(total[head].astype(BF), v) + carried[head * CHUNK : (head + 1) * CHUNK]
            )
            new = new + dot((key_end * head_of[head]).astype(BF), v, ((0,), (0,)))
        state[...] = new
        qin[at, :] = (q * jnp.exp(prefix + so_far[0])).astype(BF)
        so_far[0] = so_far[0] + prefix[CHUNK - 1 : CHUNK]

    forwarded, passed = 1, 0
    for c in range(chunks):
        recur(c)
        if c and forwarded < min(ep, 2 * per_group):
            forward(forwarded)
            forwarded += 1
            pass_on(passed)
            passed += 1

    ssend[...] = state[...].astype(BF)
    dsend[...] = jnp.where(iota(dsend.shape, 0) == 0, so_far[0], 0.0)

    def state_out(e):
        return (
            remote(ssend, srecv.at[me], st_s.at[e], st_r.at[me], ep=e),
            remote(dsend, drecv.at[me], dc_s.at[e], dc_r.at[me], ep=e),
        )

    def state_in(e):
        return (
            remote(ssend, srecv.at[e], st_s.at[e], st_r.at[e], ep=e),
            remote(dsend, drecv.at[e], dc_s.at[e], dc_r.at[e], ep=e),
        )

    for e in range(ep):
        @pl.when(e > me)
        def _():
            for copy in state_out(e):
                copy.start()

    def part_copy(g, n):
        at = pl.ds(g * group, group)
        return remote(psend.at[n, at], precv.at[n, at], fp_s.at[n, g], fp_r.at[n, g], tp=partner)

    def sum_copy(g):
        at = pl.ds(g * group, group)
        return remote(xsum.at[at], xrecv.at[at], fx_s.at[g], fx_r.at[g], tp=across)

    def back(d):
        return remote(fin.at[block(d)], ret.at[block(d)], b_s.at[d], b_r.at[d], ep=flip(me, d, ep))

    progress = [forwarded, passed]

    def advance(until, relayed):
        while progress[0] < min(until, ep):
            forward(progress[0])
            progress[0] += 1
        while progress[1] < min(relayed, ep):
            pass_on(progress[1])
            progress[1] += 1

    def experts(g):
        at = pl.ds(g * group, group)
        gate = up = None
        for n in range(tp):
            inner = slice(n * quarter, (n + 1) * quarter)
            piece = recv[n, at, :]
            a, b = dot(piece, wg[inner, :]), dot(piece, wu[inner, :])
            gate, up = (a, b) if gate is None else (gate + a, up + b)
        hidden = (gate * (1.0 / (1.0 + jnp.exp(-gate))) * up).astype(BF)

        def piece_of(c):
            return dot(hidden, wd[:, pl.ds(pl.multiple_of(c * quarter, quarter), quarter)]).astype(BF)

        for n, c in enumerate((diagonal, partner)):
            psend[n, at, :] = piece_of(c)
            part_copy(g, n).start()
        for n, c in enumerate((across, col)):
            pkeep[n, at, :] = piece_of(c)

    def pair(g):
        at = pl.ds(g * group, group)
        part_copy(g, 0).wait_recv()
        xsum[at, :] = (pkeep[0, at, :].astype(F32) + precv[0, at, :].astype(F32)).astype(BF)
        sum_copy(g).start()

    def finish(g):
        at = pl.ds(g * group, group)
        part_copy(g, 1).wait_recv()
        sum_copy(g).wait_recv()
        value = (
            pkeep[1, at, :].astype(F32) + precv[1, at, :].astype(F32) + xrecv[at, :].astype(F32)
        ).astype(BF)
        fin[at, :] = value
        if g == 0:
            ret[0:cap, :] = value[0:cap]
        for d in range(max(1, g * per_group), (g + 1) * per_group):
            back(d).start()

    def mixer_copy(n):
        return remote(msend.at[n], mprecv.at[n], mp_s.at[n], mp_r.at[n], tp=partner)

    def mixer_sum():
        return remote(mxsum, mxrecv, mx_s.at[0], mx_r.at[0], tp=across)

    def mixer_project():
        state[...] = jnp.zeros_like(state)
        for e in range(ep - 1):
            @pl.when(e < me)
            def _():
                for copy in state_in(e):
                    copy.wait_recv()
                logs = lax.dot_general(
                    drecv[e], jnp.ones(drecv.shape[1:2] + (values,), F32), (((0,), (0,)), ((), ())),
                    precision=lax.Precision.HIGHEST, preferred_element_type=F32,
                )
                state[...] = jnp.exp(logs) * state[...] + srecv[e].astype(F32)
        held = state[...]
        row = iota(held.shape, 0)
        for head in range(2):
            mine = (row < width // 2) if head == 0 else (row >= width // 2)
            cols = slice(head * values, (head + 1) * values)
            o = oloc[:, cols] + dot(qin[...], jnp.where(mine, held, 0.0).astype(BF))
            s = lax.rsqrt(jnp.mean(o * o, axis=-1, keepdims=True) + EPS)
            hn[:, cols] = (o * s * hgain_ref[head : head + 1, :]).astype(BF)
        loads[3].wait()

        def piece_of(r):
            return dot(hn[pl.ds(pl.multiple_of(r * rows_out, rows_out), rows_out), :], wo[...]).astype(BF)

        for n, r in enumerate((diagonal, partner)):
            msend[n] = piece_of(r)
            mixer_copy(n).start()
        for n, r in enumerate((across, col)):
            mkeep[n] = piece_of(r)

    def mixer_pair():
        mixer_copy(0).wait_recv()
        mxsum[...] = (mkeep[0].astype(F32) + mprecv[0].astype(F32)).astype(BF)
        mixer_sum().start()

    for load in loads[:3]:
        load.wait()
    for g in range(groups):
        first, last = g * per_group, (g + 1) * per_group
        advance(last, last)
        for d in range(first, last):
            beside_in(d).wait_recv()
            relay_in(d).wait_recv()
        experts(g)
        advance(last + per_group, last)
        pair(g)
        if g == min(1, groups - 1):
            mixer_project()
        if g == min(2, groups - 1):
            mixer_pair()
        if g:
            finish(g - 1)
    finish(groups - 1)

    mixer_copy(1).wait_recv()
    mixer_sum().wait_recv()
    out1[...] = (mkeep[1].astype(F32) + mprecv[1].astype(F32) + mxrecv[...].astype(F32)).astype(BF)

    for d in range(1, ep):
        back(d).wait_recv()
    picked = [dot(hot[choice], ret[...], ((0,), (0,))) for choice in range(2)]
    out2[...] = (picked[0] * w_ref[:, 0:1] + picked[1] * w_ref[:, 1:2]).astype(BF)

    for d in range(ep):
        if d:
            to_expert(d).wait_send()
            back(d).wait_send()
        over(d).wait_send()
        beside(d).wait_send()
        relay(d).wait_send()
    for g in range(groups):
        for n in range(2):
            part_copy(g, n).wait_send()
        sum_copy(g).wait_send()
    for n in range(2):
        mixer_copy(n).wait_send()
    mixer_sum().wait_send()
    for e in range(ep):
        @pl.when(e > me)
        def _():
            for copy in state_out(e):
                copy.wait_send()


def body(q, k, v, f, rate, factor, extra, head_gain, wo, x, x_gain, routes, weights, wg, wu, wd):
    ep, tp = lax.axis_size("ep"), lax.axis_size("tp")
    length, width = q.shape
    values = head_gain.shape[1]
    tokens, model = x.shape
    quarter = model // tp
    hidden = wg.shape[2]
    cap = 4 * tokens // ep
    slots = ep * cap
    group = min(GROUP_ROWS, slots)
    groups = slots // group
    rows_out = length // tp
    aux = jnp.concatenate([factor[:, None], extra], axis=1)
    vm, hbm = pl.BlockSpec(memory_space=pltpu.VMEM), pl.BlockSpec(memory_space=pl.ANY)
    V = pltpu.VMEM
    sem = lambda *shape: pltpu.SemaphoreType.DMA(shape)
    levels = CHUNK.bit_length() + 1
    return pl.pallas_call(
        functools.partial(kernel, ep, tp),
        out_shape=(
            jax.ShapeDtypeStruct((rows_out, model), BF),
            jax.ShapeDtypeStruct((tokens, quarter), BF),
        ),
        in_specs=[vm] * 11 + [hbm] * 4,
        out_specs=(vm, vm),
        scratch_shapes=[
            V((slots, quarter), BF), V((tp, slots, quarter), BF), V((2, slots, quarter), BF),
            V((2, slots, quarter), BF), V((2, slots, quarter), BF), V((slots, quarter), BF),
            V((slots, quarter), BF), V((slots, quarter), BF), V((slots, quarter), BF),
            V((2, slots, tokens), BF),
            V((levels * CHUNK, CHUNK), BF), V((length, 2 * values), F32), V((length, width), BF),
            V((width, values), F32), V((width, values), BF), V((ep, width, values), BF),
            V((8, width), F32), V((ep, 8, width), F32), V((length, 2 * values), BF),
            V((2, rows_out, model), BF), V((2, rows_out, model), BF), V((2, rows_out, model), BF),
            V((rows_out, model), BF), V((rows_out, model), BF),
            V(wo.shape, BF), V(wg.shape[1:], BF), V(wu.shape[1:], BF), V(wd.shape[1:], BF),
            sem(ep), sem(ep), sem(ep), sem(ep), sem(ep), sem(ep), sem(ep), sem(ep),
            sem(2, groups), sem(2, groups), sem(groups), sem(groups), sem(ep), sem(ep),
            sem(ep), sem(ep), sem(ep), sem(ep),
            sem(2), sem(2), sem(1), sem(1), sem(4),
        ],
        compiler_params=pltpu.CompilerParams(
            collective_id=0, has_side_effects=True, vmem_limit_bytes=60 * 1024 * 1024
        ),
    )(q, k, v, f, rate[None], aux, head_gain, x, x_gain[None], routes.T, weights, wo, wg, wu, wd)


def solution(mesh):
    return jax.shard_map(
        body,
        mesh=mesh,
        in_specs=(
            P("ep", "tp"),
            P("ep", "tp"),
            P("ep", "tp"),
            P("ep", "tp"),
            P("tp"),
            P("ep"),
            P("ep", "tp"),
            P("tp", None),
            P("tp", None),
            P("ep", None),
            P(),
            P("ep", None),
            P("ep", None),
            P("ep", None, "tp"),
            P("ep", None, "tp"),
            P("ep", "tp", None),
        ),
        out_specs=(P(("ep", "tp"), None), P("ep", "tp")),
        check_vma=False,
    )
```

time: 288 us -> 95.1 us (0.33)
  Pallas kernels: 0 us -> 87.3 us
  blocking collectives: 86.8 us -> 0 us
  other arithmetic: 60.8 us -> 0.71 us
  local copies, waits for them, and re-layouts: 49.7 us -> 5.88 us
  matrix products: 35.3 us -> 0 us
  waiting for transfers between devices: 32.7 us -> 0 us
  between operations: 14 us -> 0.64 us
  starting transfers between devices: 4.77 us -> 0 us
    pallas_call x0 -> x1, Pallas kernels: none -> 87.3 us  [body(): pl.pallas_call(functools.partial(kernel, ep, tp), out_shape=(jax.ShapeDty...]
    all_gather x2 -> x0, blocking collectives: 53.5 us -> none  [prefix(): lax.all_gather(part.astype(kind), axis)]
    dot_general x28 -> x0, matrix products: 35.3 us -> none  [the longest x1 12.3 us: expert_part(): jnp.einsum('sif,fd->sid', (jax.nn.silu(gate_sum) * up_sum).astype(jnp.bfl...]
    all_to_all x1 -> x0, blocking collectives: 33.3 us -> none  [expert_part(): lax.all_to_all(buffer, 'ep', split_axis=0, concat_axis=0, tiled=True)]
    reduce_sum x11 -> x0, other arithmetic: 20.1 us -> none  [the longest x8 16.4 us: advance(): jnp.sum(block_queries[:, None] * block_keys[None, :] * decays, axis=-1)]
    dynamic_slice x25 -> x0, local copies, waits for them, and re-layouts: 17.2 us -> none  [the longest x24 16.4 us: gla_blocks(): lax.scan(advance, start_state, (blocked(query_single), blocked(key_float)...]
    all_to_all x1 -> x0, waiting for transfers between devices: 16.3 us -> none  [expert_part(): lax.all_to_all(summed, 'ep', split_axis=0, concat_axis=0, tiled=True)]
    all_gather x1 -> x0, waiting for transfers between devices: 16.3 us -> none  [expert_part(): lax.all_gather(lax.all_to_all(buffer, 'ep', split_axis=0, concat_axis=0,...]
  transfers between devices with their start and end apart: 4 -> 0, of which waited for: 2 -> 0; matrix products, arithmetic and copies ran while one was open for 39% -> 0% of each run, Pallas kernels for 0% -> 0%
where the time goes in v1:
time: 95.1 us; the launch traced here: 94.5 us
  Pallas kernels  87.3 us (92%)
  local copies, waits for them, and re-layouts  5.88 us (6%)
    pallas_call x1, Pallas kernels, body(): pl.pallas_call(functools.partial(kernel, ep, tp), out_shape=(jax.ShapeDty...  87.3 us
    unnamed x3, local copies, waits for them, and re-layouts  5.02 us

profile of v1, /device:TPU:0, one launch (start us, length us, event | category | flops | bytes accessed | tf_op | source)
XLA Modules:
  0.0 94.5 jit_solution(6676202793849957832)
XLA Ops:
  0.6 0.7 pad_maximum_fusion
  1.3 1.5 %copy.24.w_ref = f32[256,2]{1,0:T(8,128)} copy(f32[256,2]{0,1:T(2,128)} %param.28) | data formatting | bytes 4096 | tf_op args[12]
  2.8 0.9 copy.23.aux_ref
  3.7 87.3 %shard_map.167 = (bf16[128,2048]{1,0:T(8,128)(2,1)}, bf16[256,512]{1,0:T(8,128)(2,1)}) custom-call(bf16[512,128]{1,0:T(8,128)(2,1)} %q_ref.1, bf16[512,128]{1,0:T(8,128)(2,1)} %k_ref.1, bf16[512,256]{1,0:T(8,128)(2,1)} %v_ref.1, bf16[512,128]{1,0:T(8,128)(2,1)} %f_ref.1, f32[1,128]{1,0:T(1,128)} %bitcast.7, f32[512,3]{1,0:T(8,128)} %copy.23.aux_ref, ...), custom_call_target="tpu_custom_call" | custom-call | tf_op jit(solution)/shard_map/pallas_call | solution.py:410
  91.0 1.9 %copy.27 = bf16[128,2048]{1,0:T(8,128)(2,1)} copy(bf16[128,2048]{1,0:T(8,128)(2,1)} %get-tuple-element.4) | data formatting | bytes 1048576
  92.9 1.7 %copy.28 = bf16[256,512]{1,0:T(8,128)(2,1)} copy(bf16[256,512]{1,0:T(8,128)(2,1)} %get-tuple-element.5) | data formatting | bytes 524288

commit v2 on v1

--- a/solution.py
+++ b/solution.py
@@ -352,12 +352,11 @@
         experts(g)
         advance(last + per_group, last)
         pair(g)
-        if g == min(1, groups - 1):
-            mixer_project()
-        if g == min(2, groups - 1):
-            mixer_pair()
         if g:
             finish(g - 1)
+        if g == min(2, groups - 1):
+            mixer_project()
+    mixer_pair()
     finish(groups - 1)
 
     mixer_copy(1).wait_recv()

time: 95.1 us -> 87 us (0.915)
  the two profiles are of different devices: /device:TPU:0 before, /device:TPU:8 now
where the time goes in v2:
time: 87 us; the launch traced here: 86.7 us
  Pallas kernels  79.5 us (91%)
  local copies, waits for them, and re-layouts  5.88 us (7%)
    pallas_call x1, Pallas kernels, body(): pl.pallas_call(functools.partial(kernel, ep, tp), out_shape=(jax.ShapeDty...  79.5 us
    unnamed x3, local copies, waits for them, and re-layouts  5.02 us

profile of v2, /device:TPU:8, one launch (start us, length us, event | category | flops | bytes accessed | tf_op | source)
XLA Modules:
  0.0 86.7 jit_solution(5465134336540867225)
XLA Ops:
  0.6 0.7 pad_maximum_fusion
  1.3 1.5 %copy.24.w_ref = f32[256,2]{1,0:T(8,128)} copy(f32[256,2]{0,1:T(2,128)} %param.28) | data formatting | bytes 4096 | tf_op args[12]
  2.8 0.9 copy.23.aux_ref
  3.7 79.5 %shard_map.167 = (bf16[128,2048]{1,0:T(8,128)(2,1)}, bf16[256,512]{1,0:T(8,128)(2,1)}) custom-call(bf16[512,128]{1,0:T(8,128)(2,1)} %q_ref.1, bf16[512,128]{1,0:T(8,128)(2,1)} %k_ref.1, bf16[512,256]{1,0:T(8,128)(2,1)} %v_ref.1, bf16[512,128]{1,0:T(8,128)(2,1)} %f_ref.1, f32[1,128]{1,0:T(1,128)} %bitcast.7, f32[512,3]{1,0:T(8,128)} %copy.23.aux_ref, ...), custom_call_target="tpu_custom_call" | custom-call | tf_op jit(solution)/shard_map/pallas_call | solution.py:409
  83.2 1.9 %copy.27 = bf16[128,2048]{1,0:T(8,128)(2,1)} copy(bf16[128,2048]{1,0:T(8,128)(2,1)} %get-tuple-element.4) | data formatting | bytes 1048576
  85.1 1.7 %copy.28 = bf16[256,512]{1,0:T(8,128)(2,1)} copy(bf16[256,512]{1,0:T(8,128)(2,1)} %get-tuple-element.5) | data formatting | bytes 524288
